TPU v7x, 32 devices: a whole 2x2x4 slice. The times are simulated.
32 devices in a mesh: grp: 2 (over y), sp: 4 (over z), tp: 4 (over x, core).
Axes of the slice: x: 2, y: 2, z: 4, core: 2. Of those that a mesh axis runs over, the one named last changes fastest.
Arguments:
- tokens: bfloat16 [3072, 2048], P(('grp', 'sp'), 'tp'), parts along dimension 0, may hold values from -6 to 6
- norm_gain: float32 [2048], replicated, may hold values from 0.1 to 1.9
- qk_gain: float32 [4, 64], replicated, may hold values from 0.7 to 5.5
- w_query_window: bfloat16 [2048, 1024], P('sp', 'tp'), may hold values from -1 to 1
- w_key_window: bfloat16 [2048, 512], P('sp', 'tp'), may hold values from -1 to 1
- w_value_window: bfloat16 [2048, 512], P('sp', 'tp'), may hold values from -0.125 to 0.125
- sink_logits: float32 [16], P('tp'), may hold values from 0 to 5
- w_query_forget: bfloat16 [2048, 1024], P('sp', 'tp'), may hold values from -1 to 1
- w_key_forget: bfloat16 [2048, 1024], P('sp', 'tp'), may hold values from -1 to 1
- w_value_forget: bfloat16 [2048, 1024], P('sp', 'tp'), may hold values from -0.125 to 0.125
- gate_cum: float32 [3072, 16], P(('grp', 'sp'), 'tp'), parts along dimension 0, as said below
- w_merge: bfloat16 [2048, 2, 2048], P('sp', None, 'tp'), may hold values from -0.125 to 0.125
- w_branch: bfloat16 [2, 1024, 2048], P(None, 'sp', 'tp'), may hold values from -0.8984375 to 0.8984375
Outputs:
- mixed: bfloat16 [3072, 2048], P(('grp', 'sp'), 'tp'), parts along dimension 0
There are 2 independent parts, one for each index of `grp`. A program takes and returns all parts, laid end to end along the dimension named above; an argument that names none is the same for every part. Nothing has to cross between parts.
Inputs may be any that keep to these rules, and one draw needn't show every extreme that they name: `gate_cum`: along positions each head's values never rise.
All inputs are finite; a program needn't handle non-finite values.
Results may differ from a plain program's by a relative error of at most 0.012.
Values may be sent and summed in bfloat16 or wider, within the bound.
A program may use at most 64 MiB of HBM per device.

v0:
```python
import math
import jax
import jax.numpy as jnp
from jax import lax
from jax.sharding import PartitionSpec as P

HEAD = 64
WINDOW = 128
epsilon = 1e-06
big_negative = -1e30


def from_behind(value, axis, by):
    size = lax.axis_size(axis)
    pairs = [(i, i + by) for i in range(size) if 0 <= i + by < size]
    return lax.ppermute(value, axis, pairs)


def head_norm(raw, gain, head_count):
    split = raw.reshape(raw.shape[0], head_count, -1)
    scaled = split * lax.rsqrt(jnp.mean(split * split, axis=-1, keepdims=True) + epsilon) * gain
    return scaled.astype(jnp.bfloat16)


def window_attend(queries, keys_ext, values_ext, sink_rows, first_pos):
    row_count, head_count, head_size = queries.shape
    group_count = keys_ext.shape[1]
    span_rows = WINDOW // 2
    block_count = row_count // span_rows
    query_blocks = queries.reshape(
        block_count, span_rows, group_count, head_count // group_count, head_size
    )
    key_blocks = jnp.concatenate(
        [
            keys_ext[lag_index * span_rows : lag_index * span_rows + row_count].reshape(
                block_count, span_rows, group_count, head_size
            )
            for lag_index in range(3)
        ],
        axis=1,
    )
    value_blocks = jnp.concatenate(
        [
            values_ext[lag_index * span_rows : lag_index * span_rows + row_count].reshape(
                block_count, span_rows, group_count, head_size
            )
            for lag_index in range(3)
        ],
        axis=1,
    )
    scores = jnp.einsum(
        "nqgrd,nkgd->ngrqk", query_blocks, key_blocks, preferred_element_type=jnp.float32
    ) * head_size ** (-0.5)
    distance = WINDOW + jnp.arange(span_rows)[:, None] - jnp.arange(3 * span_rows)[None, :]
    key_pos = (
        first_pos
        - WINDOW
        + jnp.arange(block_count)[:, None] * span_rows
        + jnp.arange(3 * span_rows)[None, :]
    )
    is_valid = ((distance >= 0) & (distance < WINDOW))[None] & (key_pos >= 0)[:, None, :]
    is_valid = is_valid[:, None, None]
    sink_grid = sink_rows.reshape(1, group_count, head_count // group_count, 1)
    row_max = jnp.maximum(jnp.max(jnp.where(is_valid, scores, big_negative), axis=-1), sink_grid)
    weights = jnp.where(is_valid, jnp.exp(scores - row_max[..., None]), 0.0)
    row_total = jnp.sum(weights, axis=-1) + jnp.exp(sink_grid - row_max)
    prob_rows = (weights / row_total[..., None]).astype(jnp.bfloat16)
    mixed_sum = jnp.einsum(
        "ngrqk,nkgd->nqgrd", prob_rows, value_blocks, preferred_element_type=jnp.float32
    )
    return mixed_sum.reshape(row_count, head_count * head_size).astype(jnp.bfloat16)


def forget_groups(groups, keys, values, gates):
    head_count, head_size = (keys.shape[1], keys.shape[2])
    gates_all = lax.all_gather(gates, "sp", axis=0, tiled=True)

    def absorber(queries, query_gate, query_pos):

        def absorb(running, block):
            row_max, row_total, mixed_sum = running
            key_rows, value_rows, key_gate, key_pos = block
            scores = jnp.einsum(
                "qhd,khd->hqk", queries, key_rows, preferred_element_type=jnp.float32
            ) * head_size ** (-0.5)
            scores = scores + query_gate.T[:, :, None] - key_gate.T[:, None, :]
            is_valid = (query_pos[:, None] >= key_pos[None, :])[None]
            new_max = jnp.maximum(
                row_max, jnp.max(jnp.where(is_valid, scores, big_negative), axis=-1)
            )
            weights = jnp.where(is_valid, jnp.exp(scores - new_max[..., None]), 0.0)
            shrink = jnp.exp(row_max - new_max)
            row_total = row_total * shrink + jnp.sum(weights, axis=-1)
            mixed_sum = mixed_sum * shrink.T[:, :, None] + jnp.einsum(
                "hqk,khd->qhd",
                weights.astype(jnp.bfloat16),
                value_rows,
                preferred_element_type=jnp.float32,
            )
            return ((new_max, row_total, mixed_sum), None)

        return absorb

    initial = tuple(
        (
            (
                jnp.full((head_count, group[0].shape[0]), big_negative, jnp.float32),
                jnp.zeros((head_count, group[0].shape[0]), jnp.float32),
                jnp.zeros((group[0].shape[0], head_count, head_size), jnp.float32),
            )
            for group in groups
        )
    )
    first_row = jnp.int32(0)
    key_rows = lax.all_gather(keys, "sp", axis=0, tiled=True)
    value_rows = lax.all_gather(values, "sp", axis=0, tiled=True)
    piece_rows = key_rows.shape[0]
    sub_rows = math.gcd(piece_rows, 2048)
    turns = piece_rows // sub_rows
    key_gate = gates_all
    key_pos = jnp.arange(piece_rows)
    blocks = (
        key_rows.reshape(turns, sub_rows, head_count, head_size),
        value_rows.reshape(turns, sub_rows, head_count, head_size),
        key_gate.reshape(turns, sub_rows, head_count),
        key_pos.reshape(turns, sub_rows),
    )
    updated = []
    for (queries, query_gate, query_pos), state in zip(groups, initial):
        absorb = absorber(queries, query_gate, query_pos)

        def advance(current):
            return lax.scan(absorb, current, blocks)[0]

        def keep(current):
            return current

        updated.append(lax.cond(first_row <= query_pos[-1], advance, keep, state))
    finals = tuple(updated)
    return [
        (mixed_sum / row_total.T[:, :, None])
        .reshape(mixed_sum.shape[0], head_count * head_size)
        .astype(jnp.bfloat16)
        for row_max, row_total, mixed_sum in finals
    ]


def on_device(
    tokens,
    norm_gain,
    qk_gain,
    w_query_window,
    w_key_window,
    w_value_window,
    sink_logits,
    w_query_forget,
    w_key_forget,
    w_value_forget,
    gate_cum,
    w_merge,
    w_branch,
):
    row_count = tokens.shape[0]
    row_offset = lax.axis_index("sp") * row_count
    gathered = lax.all_gather(tokens, "tp", axis=1, tiled=True)
    as_float = gathered.astype(jnp.float32)
    normed = (
        as_float
        * lax.rsqrt(jnp.mean(as_float * as_float, axis=-1, keepdims=True) + epsilon)
        * norm_gain
    ).astype(jnp.bfloat16)
    merge_flat = w_merge.reshape(w_merge.shape[0], -1)
    pieces = (
        lax.all_gather(w_query_window, "sp", axis=0, tiled=True),
        lax.all_gather(w_key_window, "sp", axis=0, tiled=True),
        lax.all_gather(w_value_window, "sp", axis=0, tiled=True),
        lax.all_gather(w_query_forget, "sp", axis=0, tiled=True),
        lax.all_gather(w_key_forget, "sp", axis=0, tiled=True),
        lax.all_gather(w_value_forget, "sp", axis=0, tiled=True),
        lax.all_gather(merge_flat, "sp", axis=0, tiled=True),
    )
    projected = tuple(
        (jnp.dot(normed, weight_rows, preferred_element_type=jnp.float32) for weight_rows in pieces)
    )
    query_heads = w_query_window.shape[1] // HEAD
    group_heads = w_key_window.shape[1] // HEAD
    window_query = head_norm(projected[0], qk_gain[0], query_heads)
    window_key = head_norm(projected[1], qk_gain[1], group_heads)
    window_value = projected[2].astype(jnp.bfloat16).reshape(row_count, group_heads, HEAD)
    prev_key, prev_value = from_behind(
        (window_key[row_count - WINDOW :], window_value[row_count - WINDOW :]), "sp", 1
    )
    window_out = window_attend(
        window_query,
        jnp.concatenate([prev_key, window_key], axis=0),
        jnp.concatenate([prev_value, window_value], axis=0),
        sink_logits,
        row_offset,
    )
    forget_query = head_norm(projected[3], qk_gain[2], query_heads)
    forget_key = head_norm(projected[4], qk_gain[3], query_heads)
    forget_value = projected[5].astype(jnp.bfloat16).reshape(row_count, query_heads, HEAD)
    own_pos = row_offset + jnp.arange(row_count)
    forget_out = forget_groups(
        [(forget_query, gate_cum, own_pos)], forget_key, forget_value, gate_cum
    )[0]
    channel_count = w_merge.shape[2]
    merge_gate = jax.nn.sigmoid(projected[6]).reshape(row_count, 2, channel_count)
    branch_full = lax.all_gather(w_branch, "sp", axis=1, tiled=True)
    head_stack = jnp.stack([window_out, forget_out], axis=1)
    weight_rows = branch_full
    projection = jnp.einsum(
        "uxa,xag->uxg",
        lax.all_gather(head_stack, "tp", axis=2, tiled=True),
        weight_rows,
        preferred_element_type=jnp.float32,
    )
    return (merge_gate[:, 0] * projection[:, 0] + merge_gate[:, 1] * projection[:, 1]).astype(
        jnp.bfloat16
    )


def solution(mesh):
    return jax.shard_map(
        on_device,
        mesh=mesh,
        in_specs=(
            P(("grp", "sp"), "tp"),
            P(),
            P(),
            P("sp", "tp"),
            P("sp", "tp"),
            P("sp", "tp"),
            P("tp"),
            P("sp", "tp"),
            P("sp", "tp"),
            P("sp", "tp"),
            P(("grp", "sp"), "tp"),
            P("sp", None, "tp"),
            P(None, "sp", "tp"),
        ),
        out_specs=P(("grp", "sp"), "tp"),
        check_vma=False,
    )
```

profile of v0, /device:TPU:0, one launch (start us, length us, event | category | flops | bytes accessed | tf_op | source)
XLA Modules:
  0.0 339.6 jit_solution(14842164746860835694)
XLA Ops:
  13.7 16.6 %all_gather.48 = f32[1536,4]{0,1:T(4,128)} all-gather(f32[384,4]{0,1:T(4,128)} %param.27), channel_id=1, replica_groups=mesh['grp'=2,'sp'=4,'tp'=4] {'sp'}, dimensions={0}, use_global_device_ids=true | all-gather | bytes 30720 | tf_op jit(solution)/shard_map/all_gather | solution.py:76
  30.5 19.0 %all_gather.42 = bf16[2048,128]{1,0:T(8,128)(2,1)} all-gather(bf16[512,128]{1,0:T(8,128)(2,1)S(1)} %copy-done.8), channel_id=1, replica_groups=mesh['grp'=2,'sp'=4,'tp'=4] {'sp'}, dimensions={0}, use_global_device_ids=true | all-gather | bytes 655360 | tf_op jit(solution)/shard_map/all_gather | solution.py:175
  50.2 21.1 %all_gather.41 = bf16[2048,128]{1,0:T(8,128)(2,1)} all-gather(bf16[512,128]{1,0:T(8,128)(2,1)S(1)} %copy-done.9), channel_id=1, replica_groups=mesh['grp'=2,'sp'=4,'tp'=4] {'sp'}, dimensions={0}, use_global_device_ids=true | all-gather | bytes 655360 | tf_op jit(solution)/shard_map/all_gather | solution.py:176
  74.3 2.5 multiply_reduce_fusion.1
  77.0 25.4 %all_gather.45 = bf16[1536,4,64]{0,2,1:T(8,128)(2,1)S(1)} all-gather(bf16[384,4,64]{0,2,1:T(8,128)(2,1)S(1)} %multiply_convert_fusion.2), channel_id=1, replica_groups=mesh['grp'=2,'sp'=4,'tp'=4] {'sp'}, dimensions={0}, use_global_device_ids=true | all-gather | bytes 983040 | tf_op jit(solution)/shard_map/all_gather | solution.py:115
  102.5 5.3 %all-gather.17.cloned.1.call-done = bf16[2048,256]{1,0:T(8,128)(2,1)} async-done(((bf16[512,256]{1,0:T(8,128)(2,1)}), bf16[2048,256]{1,0:T(8,128)(2,1)}) %all-gather.17.cloned.1.call-update) | async-done | bytes 1048592 | tf_op jit(solution)/shard_map/all_gather | solution.py:179
  109.7 25.2 %all_gather.47 = bf16[1536,4,64]{0,2,1:T(8,128)(2,1)S(1)} all-gather(bf16[384,4,64]{0,2,1:T(8,128)(2,1)S(1)} %bitcast.165), channel_id=1, replica_groups=mesh['grp'=2,'sp'=4,'tp'=4] {'sp'}, dimensions={0}, use_global_device_ids=true | all-gather | bytes 983040 | tf_op jit(solution)/shard_map/all_gather | solution.py:116
  134.9 8.7 %all-gather.19.cloned.1.call-done = bf16[2048,256]{1,0:T(8,128)(2,1)} async-done(((bf16[512,256]{1,0:T(8,128)(2,1)}), bf16[2048,256]{1,0:T(8,128)(2,1)}) %all-gather.19.cloned.1.call-update) | async-done | bytes 1048592 | tf_op jit(solution)/shard_map/all_gather | solution.py:177
  149.0 35.5 %conditional.1 = (f32[4,384]{1,0:T(4,128)}, f32[384,4,64]{0,2,1:T(8,128)}) conditional(s32[]{:T(128)} %bitcast.13, () %tuple.20, (bf16[1536,4,64]{0,2,1:T(8,128)(2,1)S(1)}, bf16[1536,4,64]{0,2,1:T(8,128)(2,1)S(1)}, f32[1536,4]{0,1:T(4,128)}, s32[3,512]{1,0:T(4,128)S(1)}, s32[3,512]{1,0:T(4,128)S(1)}, /*index=5*/s32[384]{0:T(512)}, ...), branch_computations={%region_7.8_spmd, %region_8.13_spmd} | conditional | flops 215199744 | bytes 15060769 | solution.py:138
  151.0 33.5 %while.18 = (s32[]{:T(128)}, f32[4,384]{1,0:T(4,128)S(1)}, f32[4,384]{1,0:T(4,128)}, f32[384,4,64]{0,2,1:T(8,128)}, s32[384]{0:T(512)}, /*index=5*/s32[3,512]{1,...) while((s32[]{:T(128)}, f32[4,384]{1,0:T(4,128)S(1)}, ...), condition=%wide.region_12.12_spmd.clone, body=%wide.region_9.11_spmd.clone.sunk | while | flops 215196672 | bytes 11896481 | solution.py:133
  153.2 2.7 fusion.85
  158.8 2.7 fusion.89
  163.8 2.7 fusion.85
  170.1 2.9 fusion.89
  175.3 2.7 fusion.85
  181.6 2.9 fusion.89
  189.8 2.8 collective-permute-start.1
  192.6 3.3 collective-permute-start
  203.8 14.9 %all-gather.23.cloned.1.call-done = bf16[2,1024,512]{2,1,0:T(8,128)(2,1)} async-done(((bf16[2,256,512]{2,1,0:T(8,128)(2,1)}), bf16[2,1024,512]{2,1,0:T(8,128)(2,1)}) %all-gather.23.cloned.1.call-update) | async-done | bytes 2097168 | tf_op jit(solution)/shard_map/all_gather | solution.py:209
  218.6 21.5 %all-gather.21.cloned.1.call-done = bf16[384,2,1024]{2,0,1:T(8,128)(2,1)} async-done(((bf16[384,2,256]{2,0,1:T(8,128)(2,1)}), bf16[384,2,1024]{2,0,1:T(8,128)(2,1)}) %all-gather.21.cloned.1.call-update) | async-done | bytes 1572880 | tf_op jit(solution)/shard_map/all_gather | solution.py:214
  240.2 3.0 convolution_bitcast_fusion
  243.2 79.3 %all-gather.11.cloned.1.call-done = bf16[2048,1024]{1,0:T(8,128)(2,1)} async-done(((bf16[512,1024]{1,0:T(8,128)(2,1)}), bf16[2048,1024]{1,0:T(8,128)(2,1)}) %all-gather.11.cloned.1.call-update) | async-done | bytes 4194320 | tf_op jit(solution)/shard_map/all_gather | solution.py:180
  322.5 5.3 %add_divide_fusion = f32[384,1024]{1,0:T(8,128)} fusion(bf16[384,2048]{1,0:T(8,128)(2,1)S(1)} %copy-done.1, bf16[2048,1024]{1,0:T(8,128)(2,1)} %all-gather.11.cloned.1.call-done), kind=kOutput, calls=%fused_computation.44 | convolution fusion | flops 1611792384 | bytes 7340032 | tf_op jit(solution)/shard_map/dot_general | solution.py:183
  327.8 2.6 reshape.258
  (143 shorter events, 51.7 us)
Async XLA Ops:
  6.5 6.6 %copy-start.15 = (f32[4,64]{1,0:T(4,128)S(1)}, f32[4,64]{1,0:T(4,128)}, u32[]{:S(2)}) copy-start(f32[4,64]{1,0:T(4,128)} %param.19) | copy-start | bytes 3076
  6.5 24.0 %copy-start.8 = (bf16[512,128]{1,0:T(8,128)(2,1)S(1)}, bf16[512,128]{1,0:T(8,128)(2,1)}, u32[]{:S(2)}) copy-start(bf16[512,128]{1,0:T(8,128)(2,1)} %param.21) | copy-start | bytes 393220
  6.5 42.9 %copy-start.16 = (f32[4]{0:T(128)S(1)}, f32[4]{0:T(128)}, u32[]{:S(2)}) copy-start(f32[4]{0:T(128)} %param.23) | copy-start | bytes 52
  6.5 43.6 %copy-start.9 = (bf16[512,128]{1,0:T(8,128)(2,1)S(1)}, bf16[512,128]{1,0:T(8,128)(2,1)}, u32[]{:S(2)}) copy-start(bf16[512,128]{1,0:T(8,128)(2,1)} %param.22) | copy-start | bytes 393220
  6.5 65.4 %all-gather.9.cloned.1.call-start = ((), (), s32[]{:S(2)}) async-start(), calls=%async_computation | async-start | bytes 1966080 | tf_op jit(solution)/shard_map/all_gather | solution.py:165
  7.3 67.1 %all-gather.15.cloned.1.call-start = ((), (), s32[]{:S(2)}) async-start(), calls=%async_computation.3 | async-start | bytes 1310720 | tf_op jit(solution)/shard_map/all_gather | solution.py:178
  8.0 99.7 %all-gather.17.cloned.1.call-start = ((), (), s32[]{:S(2)}) async-start(), calls=%async_computation.4 | async-start | bytes 1310720 | tf_op jit(solution)/shard_map/all_gather | solution.py:179
  8.8 134.9 %all-gather.19.cloned.1.call-start = ((), (), s32[]{:S(2)}) async-start(), calls=%async_computation.5 | async-start | bytes 1310720 | tf_op jit(solution)/shard_map/all_gather | solution.py:177
  9.3 176.2 %all-gather.13.cloned.1.call-start = ((), (), s32[]{:S(2)}) async-start(), calls=%async_computation.2 | async-start | bytes 1310720 | tf_op jit(solution)/shard_map/all_gather | solution.py:174
  9.9 208.7 %all-gather.23.cloned.1.call-start = ((), (), s32[]{:S(2)}) async-start(), calls=%async_computation.7 | async-start | bytes 2621440 | tf_op jit(solution)/shard_map/all_gather | solution.py:209
  10.5 63.4 %copy-start.11 = (f32[2048]{0:T(1024)S(1)}, f32[2048]{0:T(1024)}, u32[]{:S(2)}) copy-start(f32[2048]{0:T(1024)} %param.18) | copy-start | bytes 24580
  10.5 229.6 %all-gather.21.cloned.1.call-start = ((), (), s32[]{:S(2)}) async-start(), calls=%async_computation.6 | async-start | bytes 1966080 | tf_op jit(solution)/shard_map/all_gather | solution.py:214
  71.9 1.9 copy-start.2
  74.3 72.6 %copy-start = (bf16[384,2048]{1,0:T(8,128)(2,1)}, bf16[384,2048]{1,0:T(8,128)(2,1)S(1)}, u32[]{:S(2)}) copy-start(bf16[384,2048]{1,0:T(8,128)(2,1)S(1)} %fusion.27) | copy-start | bytes 4718596
  143.7 2.1 copy-start.3
  145.7 1.2 copy-start.4
  185.5 2.6 copy-start.5
  188.4 1.2 copy-start.12
  188.6 7.3 %copy-start.14 = (f32[64]{0:T(128)S(1)}, f32[64]{0:T(128)}, u32[]{:S(2)}) copy-start(f32[64]{0:T(128)} %get-tuple-element.195) | copy-start | bytes 772
  189.8 7.2 %collective-permute-start.1 = (bf16[128,2,64]{0,2,1:T(8,128)(2,1)S(1)}, bf16[128,2,64]{0,2,1:T(8,128)(2,1)S(1)}, u32[]{:S(2)}, u32[]{:S(2)}) collective-permute-start(bf16[128,2,64]{0,2,1:T(8,128)(2,1)S(1)} %slice.68), channel_id=1, source_target_pairs={{0,4},{4,8},{8,12},{1,5},{5,9},{9,13},{2,6},{6,10},{10,14},{3,7},{... | collective-permute-start | bytes 98312 | tf_op jit(solution)/shard_map/ppermute | solution.py:16
  192.6 5.4 %collective-permute-start = (bf16[128,2,64]{0,2,1:T(8,128)(2,1)S(1)}, bf16[128,2,64]{0,2,1:T(8,128)(2,1)S(1)}, u32[]{:S(2)}, u32[]{:S(2)}) collective-permute-start(bf16[128,2,64]{0,2,1:T(8,128)(2,1)S(1)} %bitcast.167), channel_id=1, source_target_pairs={{0,4},{4,8},{8,12},{1,5},{5,9},{9,13},{2,6},{6,10},{10,14},{3,7},{... | collective-permute-start | bytes 98312 | tf_op jit(solution)/shard_map/ppermute | solution.py:16
  200.9 1.5 copy-start.6
  202.4 120.1 %all-gather.11.cloned.1.call-start = ((), (), s32[]{:S(2)}) async-start(), calls=%async_computation.1 | async-start | bytes 5242880 | tf_op jit(solution)/shard_map/all_gather | solution.py:180
  203.8 118.7 %copy-start.1 = (bf16[384,2048]{1,0:T(8,128)(2,1)S(1)}, bf16[384,2048]{1,0:T(8,128)(2,1)}, u32[]{:S(2)}) copy-start(bf16[384,2048]{1,0:T(8,128)(2,1)} %copy-done) | copy-start | bytes 4718596
  (3 other events, 3.0 us)
Sparse Core Ops, SparseCore 0:
  8.9 22.3 all-gather.8
  32.9 36.9 all-gather.14
  71.5 36.1 all-gather.16
  109.1 34.4 all-gather.18
  145.1 27.0 all-gather.12
  173.6 45.0 all-gather.22
  220.2 19.9 all-gather.20
  241.7 80.7 all-gather.10
where the time goes:
time: 341 us; the launch traced here: 340 us
  waiting for transfers between devices  134 us (39%)
  blocking collectives  107 us (31%)
  matrix products  37.9 us (11%)
  other arithmetic  23.1 us (7%)
  local copies, waits for them, and re-layouts  16.3 us (5%)
  between operations  14.7 us (4%)
  starting transfers between devices  6.38 us (2%)
    all_gather x1, waiting for transfers between devices, on_device(): lax.all_gather(merge_flat, 'sp', axis=0, tiled=True)  79.3 us
    all_gather x1, blocking collectives, forget_groups(): key_rows = lax.all_gather(keys, 'sp', axis=0, tiled=True)  25.4 us
    all_gather x1, blocking collectives, forget_groups(): value_rows = lax.all_gather(values, 'sp', axis=0, tiled=True)  25.2 us
    all_gather x1, waiting for transfers between devices, on_device(): lax.all_gather(head_stack, 'tp', axis=2, tiled=True)  21.5 us
    all_gather x1, blocking collectives, on_device(): lax.all_gather(w_value_window, 'sp', axis=0, tiled=True)  21.1 us
    all_gather x1, blocking collectives, on_device(): lax.all_gather(w_key_window, 'sp', axis=0, tiled=True)  19 us
    dot_general x7, matrix products, on_device(): jnp.dot(normed, weight_rows, preferred_element_type=jnp.float32)  16.8 us
    all_gather x1, blocking collectives, forget_groups(): gates_all = lax.all_gather(gates, 'sp', axis=0, tiled=True)  16.6 us
  transfers between devices with their start and end apart: 10, of which 6 were waited for; matrix products, arithmetic and copies ran while one was open for 20% of the time, Pallas kernels for 0%

commit v1 on v0

--- a/solution.py
+++ b/solution.py
@@ -1,3 +1,4 @@
+import functools
 import math
 import jax
 import jax.numpy as jnp
@@ -8,6 +9,27 @@
 WINDOW = 128
 epsilon = 1e-06
 big_negative = -1e30
+
+
+def _part_table(target, shard_axis):
+    num = lax.axis_size(shard_axis)
+    store = []
+    h = 0
+    while h < num:
+        store.append((h, (h + 1) % num))
+        h += 1
+    back = [None] * num
+    back[num - 1] = target
+    for m in range(num - 2, -1, -1):
+        back[m] = lax.ppermute(back[m + 1], shard_axis, perm=store)
+    top = jnp.concatenate(back, 0)
+    moved = lax.axis_index(shard_axis)
+    passed = (moved + 1) * target.shape[0]
+    front = jnp.roll(top, passed, 0)
+    return front
+
+
+meet_lane_here = functools.partial(_part_table, shard_axis="sp")
 
 
 def from_behind(value, axis, by):
@@ -113,7 +135,7 @@
     )
     first_row = jnp.int32(0)
     key_rows = lax.all_gather(keys, "sp", axis=0, tiled=True)
-    value_rows = lax.all_gather(values, "sp", axis=0, tiled=True)
+    value_rows = meet_lane_here(values)
     piece_rows = key_rows.shape[0]
     sub_rows = math.gcd(piece_rows, 2048)
     turns = piece_rows // sub_rows

time: 341 us -> 370 us (1.085)
  waiting for transfers between devices: 134 us -> 169 us
  blocking collectives: 107 us -> 82.5 us
  local copies, waits for them, and re-layouts: 16.3 us -> 25.8 us
  starting transfers between devices: 6.38 us -> 10.7 us
    all_gather x1, waiting for transfers between devices: 0.02 us -> 25.7 us  [on_device(): lax.all_gather(w_query_window, 'sp', axis=0, tiled=True)]
    all_gather x1 -> x0, blocking collectives: 25.2 us -> none  [forget_groups(): value_rows = lax.all_gather(values, 'sp', axis=0, tiled=True)]
    ppermute x0 -> x3, waiting for transfers between devices: none -> 24.3 us  [_part_table(): back[m] = lax.ppermute(back[m + 1], shard_axis, perm=store)]
    all_gather x1, waiting for transfers between devices: 14.9 us -> 0.02 us  [on_device(): branch_full = lax.all_gather(w_branch, 'sp', axis=1, tiled=True)]
  transfers between devices with their start and end apart: 10 -> 13, of which waited for: 6 -> 7; matrix products, arithmetic and copies ran while one was open for 20% -> 22% of each run, Pallas kernels for 0% -> 0%
where the time goes in v1:
time: 370 us; the launch traced here: 368 us
  waiting for transfers between devices  169 us (46%)
  blocking collectives  82.5 us (22%)
  matrix products  39.1 us (11%)
  other arithmetic  26.1 us (7%)
  local copies, waits for them, and re-layouts  25.8 us (7%)
  between operations  14.7 us (4%)
  starting transfers between devices  10.7 us (3%)
    all_gather x1, waiting for transfers between devices, on_device(): lax.all_gather(merge_flat, 'sp', axis=0, tiled=True)  79.3 us
    all_gather x1, waiting for transfers between devices, on_device(): lax.all_gather(w_query_window, 'sp', axis=0, tiled=True)  25.7 us
    all_gather x1, blocking collectives, forget_groups(): key_rows = lax.all_gather(keys, 'sp', axis=0, tiled=True)  25.7 us
    ppermute x3, waiting for transfers between devices, _part_table(): back[m] = lax.ppermute(back[m + 1], shard_axis, perm=store)  24.3 us
    all_gather x1, waiting for transfers between devices, on_device(): lax.all_gather(head_stack, 'tp', axis=2, tiled=True)  22.5 us
    all_gather x1, blocking collectives, on_device(): lax.all_gather(w_value_window, 'sp', axis=0, tiled=True)  22 us
    all_gather x1, blocking collectives, on_device(): lax.all_gather(w_key_window, 'sp', axis=0, tiled=True)  18.2 us
    dot_general x7, matrix products, on_device(): jnp.dot(normed, weight_rows, preferred_element_type=jnp.float32)  17.1 us
  transfers between devices with their start and end apart: 13, of which 7 were waited for; matrix products, arithmetic and copies ran while one was open for 22% of the time, Pallas kernels for 0%

profile of v1, /device:TPU:0, one launch (start us, length us, event | category | flops | bytes accessed | tf_op | source)
XLA Modules:
  0.0 368.2 jit_solution(18147958280688204084)
XLA Ops:
  13.6 16.6 %all_gather.44 = f32[1536,4]{0,1:T(4,128)} all-gather(f32[384,4]{0,1:T(4,128)} %param.27), channel_id=1, replica_groups=mesh['grp'=2,'sp'=4,'tp'=4] {'sp'}, dimensions={0}, use_global_device_ids=true | all-gather | bytes 30720 | tf_op jit(solution)/shard_map/all_gather | solution.py:98
  30.3 18.2 %all_gather.39 = bf16[2048,128]{1,0:T(8,128)(2,1)} all-gather(bf16[512,128]{1,0:T(8,128)(2,1)S(1)} %copy-done.13), channel_id=1, replica_groups=mesh['grp'=2,'sp'=4,'tp'=4] {'sp'}, dimensions={0}, use_global_device_ids=true | all-gather | bytes 655360 | tf_op jit(solution)/shard_map/all_gather | solution.py:197
  49.2 22.0 %all_gather.38 = bf16[2048,128]{1,0:T(8,128)(2,1)} all-gather(bf16[512,128]{1,0:T(8,128)(2,1)S(1)} %copy-done.14), channel_id=1, replica_groups=mesh['grp'=2,'sp'=4,'tp'=4] {'sp'}, dimensions={0}, use_global_device_ids=true | all-gather | bytes 655360 | tf_op jit(solution)/shard_map/all_gather | solution.py:198
  77.0 25.7 %all_gather.42 = bf16[1536,4,64]{0,2,1:T(8,128)(2,1)S(1)} all-gather(bf16[384,4,64]{0,2,1:T(8,128)(2,1)S(1)} %multiply_convert_fusion.2), channel_id=1, replica_groups=mesh['grp'=2,'sp'=4,'tp'=4] {'sp'}, dimensions={0}, use_global_device_ids=true | all-gather | bytes 983040 | tf_op jit(solution)/shard_map/all_gather | solution.py:137
  102.7 5.0 %all-gather.17.cloned.1.call-done = bf16[2048,256]{1,0:T(8,128)(2,1)} async-done(((bf16[512,256]{1,0:T(8,128)(2,1)}), bf16[2048,256]{1,0:T(8,128)(2,1)}) %all-gather.17.cloned.1.call-update) | async-done | bytes 1048592 | tf_op jit(solution)/shard_map/all_gather | solution.py:201
  110.6 25.7 %all-gather.13.cloned.1.call-done = bf16[2048,256]{1,0:T(8,128)(2,1)} async-done(((bf16[512,256]{1,0:T(8,128)(2,1)}), bf16[2048,256]{1,0:T(8,128)(2,1)}) %all-gather.13.cloned.1.call-update) | async-done | bytes 1048592 | tf_op jit(solution)/shard_map/all_gather | solution.py:196
  145.1 4.0 %collective-permute-start.1 = (bf16[128,2,64]{0,2,1:T(8,128)(2,1)}, bf16[128,2,64]{0,2,1:T(8,128)(2,1)}, u32[]{:S(2)}, u32[]{:S(2)}) collective-permute-start(bf16[128,2,64]{0,2,1:T(8,128)(2,1)} %slice.68), channel_id=1, source_target_pairs={{0,4},{4,8},{8,12},{1,5},{5,9},{9,13},{2,6},{6,10},{10,14},{3,7},{... | collective-permute-start | bytes 98312 | tf_op jit(solution)/shard_map/ppermute | solution.py:38
  151.3 2.8 collective-permute-start
  156.6 8.5 %all-gather.19.cloned.1.call-done = bf16[2048,256]{1,0:T(8,128)(2,1)} async-done(((bf16[512,256]{1,0:T(8,128)(2,1)}), bf16[2048,256]{1,0:T(8,128)(2,1)}) %all-gather.19.cloned.1.call-update) | async-done | bytes 1048592 | tf_op jit(solution)/shard_map/all_gather | solution.py:199
  176.8 11.7 %collective-permute-done.3 = bf16[384,4,64]{0,2,1:T(8,128)(2,1)S(1)} collective-permute-done((bf16[384,4,64]{0,2,1:T(8,128)(2,1)}, bf16[384,4,64]{0,2,1:T(8,128)(2,1)S(1)}, u32[]{:S(2)}, u32[]{:S(2)}) %collective-permute-start.3) | collective-permute-done | bytes 196640 | tf_op jit(solution)/shard_map/ppermute | solution.py:24
  192.1 12.6 %collective-permute-done.4 = bf16[384,4,64]{0,2,1:T(8,128)(2,1)S(1)} collective-permute-done((bf16[384,4,64]{0,2,1:T(8,128)(2,1)S(1)}, bf16[384,4,64]{0,2,1:T(8,128)(2,1)S(1)}, u32[]{:S(2)}, u32[]{:S(2)}) %collective-permute-start.4) | collective-permute-done | bytes 196640 | tf_op jit(solution)/shard_map/ppermute | solution.py:24
  207.0 35.9 %conditional.1 = (f32[4,384]{1,0:T(4,128)}, f32[384,4,64]{0,2,1:T(8,128)}) conditional(s32[]{:T(128)} %bitcast.13, () %tuple.29, (bf16[1536,4,64]{0,2,1:T(8,128)(2,1)S(1)}, s32[]{:T(128)}, bf16[3072,4,64]{0,2,1:T(8,128)(2,1)S(1)}, f32[1536,4]{0,1:T(4,128)}, s32[3,512]{1,0:T(4,128)S(1)}, /*index=5*/s32[3,512]{1,0:T(4,128)S(1)}, s32[384]{0:T(512)}, ...), branch_computations={%region_7.8_spmd, %region_8.13_spmd} | conditional | flops 215199760 | bytes 16633765 | solution.py:160
  209.4 33.4 %while.26 = (s32[]{:T(128)}, f32[4,384]{1,0:T(4,128)S(1)}, f32[4,384]{1,0:T(4,128)}, f32[384,4,64]{0,2,1:T(8,128)}, s32[384]{0:T(512)}, /*index=5*/s32[3,512]{1,...) while((s32[]{:T(128)}, f32[4,384]{1,0:T(4,128)S(1)}, ...), condition=%wide.region_12.12_spmd.clone, body=%wide.region_9.11_spmd.clone.sunk | while | flops 215196672 | bytes 11896481 | solution.py:155
  211.7 2.7 fusion.85
  217.3 2.7 fusion.89
  222.3 2.7 fusion.85
  228.6 2.9 fusion.89
  233.7 2.7 fusion.85
  240.0 2.9 fusion.89
  246.3 22.5 %all-gather.21.cloned.1.call-done = bf16[384,2,1024]{2,0,1:T(8,128)(2,1)} async-done(((bf16[384,2,256]{2,0,1:T(8,128)(2,1)}), bf16[384,2,1024]{2,0,1:T(8,128)(2,1)}) %all-gather.21.cloned.1.call-update) | async-done | bytes 1572880 | tf_op jit(solution)/shard_map/all_gather | solution.py:236
  268.8 3.0 convolution_bitcast_fusion
  271.9 79.3 %all-gather.11.cloned.1.call-done = bf16[2048,1024]{1,0:T(8,128)(2,1)} async-done(((bf16[512,1024]{1,0:T(8,128)(2,1)}), bf16[2048,1024]{1,0:T(8,128)(2,1)}) %all-gather.11.cloned.1.call-update) | async-done | bytes 4194320 | tf_op jit(solution)/shard_map/all_gather | solution.py:202
  351.2 5.3 %add_divide_fusion = f32[384,1024]{1,0:T(8,128)} fusion(bf16[384,2048]{1,0:T(8,128)(2,1)S(1)} %copy-done.1, bf16[2048,1024]{1,0:T(8,128)(2,1)} %all-gather.11.cloned.1.call-done), kind=kOutput, calls=%fused_computation.45 | convolution fusion | flops 1611792384 | bytes 7340032 | tf_op jit(solution)/shard_map/dot_general | solution.py:205
  356.5 2.6 reshape.264
  (165 shorter events, 71.3 us)
Async XLA Ops:
  6.5 23.8 %copy-start.13 = (bf16[512,128]{1,0:T(8,128)(2,1)S(1)}, bf16[512,128]{1,0:T(8,128)(2,1)}, u32[]{:S(2)}) copy-start(bf16[512,128]{1,0:T(8,128)(2,1)} %param.21) | copy-start | bytes 393220
  6.5 42.0 %copy-start.20 = (f32[4]{0:T(128)S(1)}, f32[4]{0:T(128)}, u32[]{:S(2)}) copy-start(f32[4]{0:T(128)} %param.23) | copy-start | bytes 52
  6.5 42.6 %copy-start.14 = (bf16[512,128]{1,0:T(8,128)(2,1)S(1)}, bf16[512,128]{1,0:T(8,128)(2,1)}, u32[]{:S(2)}) copy-start(bf16[512,128]{1,0:T(8,128)(2,1)} %param.22) | copy-start | bytes 393220
  6.5 65.4 %all-gather.9.cloned.1.call-start = ((), (), s32[]{:S(2)}) async-start(), calls=%async_computation | async-start | bytes 1966080 | tf_op jit(solution)/shard_map/all_gather | solution.py:187
  7.3 67.0 %all-gather.15.cloned.1.call-start = ((), (), s32[]{:S(2)}) async-start(), calls=%async_computation.3 | async-start | bytes 1310720 | tf_op jit(solution)/shard_map/all_gather | solution.py:200
  8.0 99.7 %all-gather.17.cloned.1.call-start = ((), (), s32[]{:S(2)}) async-start(), calls=%async_computation.4 | async-start | bytes 1310720 | tf_op jit(solution)/shard_map/all_gather | solution.py:201
  8.8 127.5 %all-gather.13.cloned.1.call-start = ((), (), s32[]{:S(2)}) async-start(), calls=%async_computation.2 | async-start | bytes 1310720 | tf_op jit(solution)/shard_map/all_gather | solution.py:196
  9.3 155.8 %all-gather.19.cloned.1.call-start = ((), (), s32[]{:S(2)}) async-start(), calls=%async_computation.5 | async-start | bytes 1310720 | tf_op jit(solution)/shard_map/all_gather | solution.py:199
  9.9 236.4 %all-gather.23.cloned.1.call-start = ((), (), s32[]{:S(2)}) async-start(), calls=%async_computation.7 | async-start | bytes 2621440 | tf_op jit(solution)/shard_map/all_gather | solution.py:231
  10.5 63.3 %copy-start.15 = (f32[2048]{0:T(1024)S(1)}, f32[2048]{0:T(1024)}, u32[]{:S(2)}) copy-start(f32[2048]{0:T(1024)} %param.18) | copy-start | bytes 24580
  10.5 258.3 %all-gather.21.cloned.1.call-start = ((), (), s32[]{:S(2)}) async-start(), calls=%async_computation.6 | async-start | bytes 1966080 | tf_op jit(solution)/shard_map/all_gather | solution.py:236
  74.3 90.8 %copy-start = (bf16[384,2048]{1,0:T(8,128)(2,1)}, bf16[384,2048]{1,0:T(8,128)(2,1)S(1)}, u32[]{:S(2)}) copy-start(bf16[384,2048]{1,0:T(8,128)(2,1)S(1)} %fusion.27) | copy-start | bytes 4718596
  109.7 65.6 %collective-permute-start.2 = (bf16[384,4,64]{0,2,1:T(8,128)(2,1)S(1)}, bf16[384,4,64]{0,2,1:T(8,128)(2,1)}, u32[]{:S(2)}, u32[]{:S(2)}) collective-permute-start(bf16[384,4,64]{0,2,1:T(8,128)(2,1)S(1)} %bitcast.162), channel_id=1, source_target_pairs={{0,4},{4,8},{8,12},{12,0},{1,5},{5,9},{9,13},{13,1},{2,6},{6,10},{... | collective-permute-start | bytes 589832 | tf_op jit(solution)/shard_map/ppermute | solution.py:24
  145.1 23.7 %collective-permute-start.1 = (bf16[128,2,64]{0,2,1:T(8,128)(2,1)}, bf16[128,2,64]{0,2,1:T(8,128)(2,1)}, u32[]{:S(2)}, u32[]{:S(2)}) collective-permute-start(bf16[128,2,64]{0,2,1:T(8,128)(2,1)} %slice.68), channel_id=1, source_target_pairs={{0,4},{4,8},{8,12},{1,5},{5,9},{9,13},{2,6},{6,10},{10,14},{3,7},{... | collective-permute-start | bytes 98312 | tf_op jit(solution)/shard_map/ppermute | solution.py:38
  151.3 19.6 %collective-permute-start = (bf16[128,2,64]{0,2,1:T(8,128)(2,1)}, bf16[128,2,64]{0,2,1:T(8,128)(2,1)}, u32[]{:S(2)}, u32[]{:S(2)}) collective-permute-start(bf16[128,2,64]{0,2,1:T(8,128)(2,1)} %bitcast.1), channel_id=1, source_target_pairs={{0,4},{4,8},{8,12},{1,5},{5,9},{9,13},{2,6},{6,10},{10,14},{3,7},{... | collective-permute-start | bytes 98312 | tf_op jit(solution)/shard_map/ppermute | solution.py:38
  156.6 10.5 %copy-start.19 = (f32[64]{0:T(128)S(1)}, f32[64]{0:T(128)}, u32[]{:S(2)}) copy-start(f32[64]{0:T(128)} %get-tuple-element.294) | copy-start | bytes 772
  156.6 12.2 %copy-start.8 = (bf16[384,2,64]{0,2,1:T(8,128)(2,1)S(1)}, bf16[384,2,64]{0,2,1:T(8,128)(2,1)}, u32[]{:S(2)}) copy-start(bf16[384,2,64]{0,2,1:T(8,128)(2,1)} %copy-done.7) | copy-start | bytes 294916
  174.6 15.3 %copy-start.11 = (bf16[6,64,2,64]{1,3,2,0:T(8,128)(2,1)S(1)}, bf16[6,64,2,64]{1,3,2,0:T(8,128)(2,1)}, u32[]{:S(2)}) copy-start(bf16[6,64,2,64]{1,3,2,0:T(8,128)(2,1)} %copy.34) | copy-start | bytes 294916
  174.6 15.3 %copy-start.12 = (bf16[6,64,2,64]{1,3,2,0:T(8,128)(2,1)S(1)}, bf16[6,64,2,64]{1,3,2,0:T(8,128)(2,1)}, u32[]{:S(2)}) copy-start(bf16[6,64,2,64]{1,3,2,0:T(8,128)(2,1)} %copy.33) | copy-start | bytes 294916
  175.3 13.2 %collective-permute-start.3 = (bf16[384,4,64]{0,2,1:T(8,128)(2,1)}, bf16[384,4,64]{0,2,1:T(8,128)(2,1)S(1)}, u32[]{:S(2)}, u32[]{:S(2)}) collective-permute-start(bf16[384,4,64]{0,2,1:T(8,128)(2,1)} %collective-permute-done.2), channel_id=1, source_target_pairs={{0,4},{4,8},{8,12},{12,0},{1,5},{5,9},{9,13},{13,1},{2,6},{6,10},{... | collective-permute-start | bytes 589832 | tf_op jit(solution)/shard_map/ppermute | solution.py:24
  188.5 16.2 %collective-permute-start.4 = (bf16[384,4,64]{0,2,1:T(8,128)(2,1)S(1)}, bf16[384,4,64]{0,2,1:T(8,128)(2,1)S(1)}, u32[]{:S(2)}, u32[]{:S(2)}) collective-permute-start(bf16[384,4,64]{0,2,1:T(8,128)(2,1)S(1)} %collective-permute-done.3), channel_id=1, source_target_pairs={{0,4},{4,8},{8,12},{12,0},{1,5},{5,9},{9,13},{13,1},{2,6},{6,10},{... | collective-permute-start | bytes 589832 | tf_op jit(solution)/shard_map/ppermute | solution.py:24
  207.0 37.2 %copy-start.6 = (bf16[384,1,256]{2,0,1:T(8,128)(2,1)S(1)}, bf16[384,1,256]{2,0,1:T(8,128)(2,1)}, u32[]{:S(2)}) copy-start(bf16[384,1,256]{2,0,1:T(8,128)(2,1)} %convert_element_type.84) | copy-start | bytes 589828
  244.9 106.2 %all-gather.11.cloned.1.call-start = ((), (), s32[]{:S(2)}) async-start(), calls=%async_computation.1 | async-start | bytes 5242880 | tf_op jit(solution)/shard_map/all_gather | solution.py:202
  246.3 104.9 %copy-start.1 = (bf16[384,2048]{1,0:T(8,128)(2,1)S(1)}, bf16[384,2048]{1,0:T(8,128)(2,1)}, u32[]{:S(2)}) copy-start(bf16[384,2048]{1,0:T(8,128)(2,1)} %copy-done) | copy-start | bytes 4718596
  (10 other events, 49.5 us)
Sparse Core Ops, SparseCore 0:
  8.9 22.3 all-gather.8
  32.9 37.8 all-gather.14
  72.3 35.3 all-gather.16
  109.1 27.1 all-gather.12
  137.7 27.3 all-gather.18
  166.5 55.1 all-gather.22
  245.1 23.7 all-gather.20
  270.4 80.7 all-gather.10
